TPU v7x, 768 devices: a whole 4x8x12 slice. The times are simulated.
768 devices in a mesh: sp: 384 (over z, y, x), tp: 2 (over core).
Axes of the slice: x: 4, y: 8, z: 12, core: 2. Of those that a mesh axis runs over, the one named last changes fastest.
Arguments:
- tokens: bfloat16 [98304, 2048], P('sp'), may hold values from -6 to 6
- query_weight: bfloat16 [2, 2048, 512], P(None, None, 'tp'), may hold values from -0.125 to 0.125
- key_weight: bfloat16 [2, 2048, 512], P(None, None, 'tp'), may hold values from -0.125 to 0.125
- value_weight: bfloat16 [2, 2048, 512], P(None, None, 'tp'), may hold values from -0.125 to 0.125
- out_weight: bfloat16 [2, 512, 2048], replicated, may hold values from -1.5 to 1.5
- rel_table: float32 [2, 8, 257], P(None, 'tp'), may hold values from -5 to 262
- norm_gain: float32 [2, 2048], replicated, may hold values from 0.1 to 1.9
- norm_bias: float32 [2, 2048], replicated, may hold values from -1.5 to 1.5
Outputs:
- encoded: bfloat16 [98304, 2048], P('sp', 'tp')
All inputs are finite; a program needn't handle non-finite values.
Results may differ from a plain program's by a relative error of at most 0.0095.
Values may be sent and summed in bfloat16 or wider, within the bound.
No kernel may reach another device: no remote copies, remote signals or barrier semaphores. Data moves between devices by JAX's collectives and lax.ppermute only.
A program may use at most 64 MiB of HBM per device.

v0:
```python
import functools

import jax
import jax.numpy as jnp
from jax import lax
from jax.experimental import pallas as pl
from jax.experimental.pallas import tpu as pltpu
from jax.sharding import PartitionSpec as P

SEG = 64
LEFT = 4
CLIP = 128
LAYERS = 2
REACH = LEFT * SEG
BAND = REACH + SEG
SPAN = 384

residual_scale = 2.0**0.5
norm_eps = 1e-05
masked_score = -1e30

VM = pl.BlockSpec(memory_space=pltpu.VMEM)
ANY = pl.BlockSpec(memory_space=pltpu.HBM)
bf16 = jnp.bfloat16
f32 = jnp.float32


def kernel_call(body, outs, specs, args, scratch=(), limit=10 << 20, flops=10**9, out_specs=None):
    return pl.pallas_call(
        body,
        out_shape=[jax.ShapeDtypeStruct(s, d) for s, d in outs],
        in_specs=specs,
        out_specs=out_specs or [VM] * len(outs),
        scratch_shapes=scratch,
        compiler_params=pltpu.CompilerParams(vmem_limit_bytes=limit),
        cost_estimate=pl.CostEstimate(flops=flops, transcendentals=0, bytes_accessed=1 << 20),
    )(*args)


def is_late(position):
    even = jnp.logical_and(lax.rem(position, 2) == 0, position > 0)
    return jnp.logical_or(even, position == 1)


def late_position(position):
    return position == 1 or (position % 2 == 0 and position > 0)


def matmul(a, b):
    return jnp.dot(a, b, preferred_element_type=f32)


def when_class(late, run):
    flag = is_late(lax.axis_index("sp"))
    pl.when(flag if late else jnp.logical_not(flag))(run)


def fetch(pairs, sem):
    copies = [pltpu.make_async_copy(a, b, sem.at[i]) for i, (a, b) in enumerate(pairs)]
    for copy in copies:
        copy.start()
    return copies


def first_kv(late, tok, wk, wv, kv, tokv, wks, wvs, sem):
    def run():
        _, width = tok.shape
        heads = wk.shape[2]
        parts = sem.shape[1]
        step = width // parts
        copies = []
        for c in range(parts):
            cut = pl.ds(c * step, step)
            trio = (
                pltpu.make_async_copy(tok.at[:, cut], tokv.at[:, cut], sem.at[0, c]),
                pltpu.make_async_copy(wk.at[0, cut, :], wks.at[cut, :], sem.at[1, c]),
                pltpu.make_async_copy(wv.at[0, cut, :], wvs.at[cut, :], sem.at[2, c]),
            )
            for copy in trio:
                copy.start()
            copies.append(trio)
        keys = values = None
        for c in range(parts):
            for copy in copies[c]:
                copy.wait()
            cut = pl.ds(c * step, step)
            x = tokv[:, cut]
            k = matmul(x, wks[cut, :])
            v = matmul(x, wvs[cut, :])
            keys = k if keys is None else keys + k
            values = v if values is None else values + v
        kv[:, :heads] = keys.astype(bf16)
        kv[:, heads:] = values.astype(bf16)

    when_class(late, run)


def fill_bias(table, bias):
    rows, cols = table.shape
    t = table[...]
    head = t[:, : cols - 1]
    offset = lax.broadcasted_iota(jnp.int32, (cols - 1, SPAN), 1)
    index = lax.broadcasted_iota(jnp.int32, (cols - 1, SPAN), 0)
    onehot = (jnp.clip(REACH + SEG - 1 - offset, -CLIP, CLIP) + CLIP == index).astype(f32).astype(bf16)
    high = head.astype(bf16)
    rest = head - high.astype(f32)
    mid = rest.astype(bf16)
    low = (rest - mid.astype(f32)).astype(bf16)
    by_offset = matmul(high, onehot) + matmul(mid, onehot) + matmul(low, onehot)
    far = lax.broadcasted_iota(jnp.int32, (rows, SPAN), 1) <= REACH + SEG - 1 - CLIP
    by_offset = jnp.where(far, t[:, cols - 1 :], by_offset)
    for r in range(rows):
        line = jnp.broadcast_to(by_offset[r : r + 1, :], (SEG, SPAN))
        skew = pltpu.roll(line, SPAN - (SEG - 1), 1, stride=1, stride_axis=0)
        bias[r * SEG : (r + 1) * SEG, :] = skew


def scaled_query(x, w):
    return (matmul(x, w).astype(bf16).astype(f32) * 0.125).astype(bf16)


def choose(main, late, out):
    def from_main():
        out[...] = main[...]

    def from_late():
        out[...] = late[...]

    when_class(False, from_main)
    when_class(True, from_late)


def first_query(layer, x_main, x_late, wq, wo, wk, wv, table, q, bias, x, wo0, wk1, wv1, wqs, sem):
    copies = fetch(
        ((wq.at[layer], wqs), (wo.at[layer], wo0), (wk.at[layer + 1], wk1), (wv.at[layer + 1], wv1)), sem
    )
    choose(x_main, x_late, x)
    fill_bias(table, bias)
    copies[0].wait()
    q[...] = scaled_query(x[...], wqs[...])
    for copy in copies[1:]:
        copy.wait()


def later_query(layer, x_main, x_late, wq, wo, q, x, wo1, wqs, sem):
    copies = fetch(((wq.at[layer], wqs), (wo.at[layer], wo1)), sem)
    choose(x_main, x_late, x)
    copies[0].wait()
    q[...] = scaled_query(x[...], wqs[...])
    copies[1].wait()


def attend(layer, q, bias, ext, out):
    rows, width = q.shape
    heads = width // 64
    lane = lax.broadcasted_iota(jnp.int32, (SEG, width), 1) // 64
    column = lax.broadcasted_iota(jnp.int32, (1, BAND), 1)
    blocked = jnp.where(lax.axis_index("sp") == 0, masked_score, 0.0)
    for i in range(rows // SEG):
        qs = q[i * SEG : (i + 1) * SEG, :]
        stack = jnp.concatenate(
            [jnp.where(lane == h, qs, jnp.zeros_like(qs)) for h in range(heads)], axis=0
        )
        keys = ext[i * SEG : i * SEG + BAND, :width]
        values = ext[i * SEG : i * SEG + BAND, width:]
        score = lax.dot_general(stack, keys, (((1,), (1,)), ((), ())), preferred_element_type=f32)
        score = score + bias[layer * heads * SEG : (layer + 1) * heads * SEG, :BAND]
        score = score + jnp.where(column < REACH - i * SEG, blocked, 0.0)
        peak = jnp.max(score, -1, keepdims=True)
        expo = jnp.exp(score - peak)
        scale = 1.0 / jnp.sum(expo, -1, keepdims=True)
        mixed = matmul(expo.astype(bf16), values) * scale
        total = None
        for h in range(heads):
            part = jnp.where(lane == h, mixed[h * SEG : (h + 1) * SEG, :], 0.0)
            total = part if total is None else total + part
        out[i * SEG : (i + 1) * SEG, :] = total.astype(bf16)


def choose_source(main, late, out):
    late_source = is_late(lax.axis_index("sp") - 1)

    @pl.when(late_source)
    def _():
        out[...] = late[...]

    @pl.when(jnp.logical_not(late_source))
    def _():
        out[...] = main[...]


def main_attention(layer, q, own, prev, bias, out, ext):
    def run():
        rows = q.shape[0]
        ext[:rows, :] = prev[...]
        ext[rows:, :] = own[...]
        attend(layer, q, bias, ext, out)

    when_class(False, run)


def late_attention(layer, q, own, prev_main, prev_late, bias, out, ext):
    def run():
        rows = q.shape[0]
        choose_source(prev_main, prev_late, ext.at[:rows, :])
        ext[rows:, :] = own[...]
        attend(layer, q, bias, ext, out)

    when_class(True, run)


def final_attention(layer, q, own_main, own_late, prev_main, prev_late, bias, out, ext):
    rows = q.shape[0]
    choose(own_main, own_late, ext.at[rows:, :])
    choose_source(prev_main, prev_late, ext.at[:rows, :])
    attend(layer, q, bias, ext, out)


def out_project(att, wo, x, total):
    width = x.shape[1]
    step = 512
    count = width // step
    a = att[...]
    means, squares = [], []
    for c in range(count):
        cut = slice(c * step, (c + 1) * step)
        t = residual_scale * x[:, cut].astype(f32) + matmul(a, wo[:, cut])
        total[:, cut] = t
        m = jnp.sum(t, -1, keepdims=True) * (1.0 / step)
        d = t - m
        means.append(m)
        squares.append(jnp.sum(d * d, -1, keepdims=True))
    mean = sum(means) * (1.0 / count)
    square = sum(squares) + step * sum((m - mean) * (m - mean) for m in means)
    return mean, lax.rsqrt(square * (1.0 / width) + norm_eps)


def middle(late, layer, att, wo, x, gain, shift, wk, wv, y, kv, total):
    def run():
        width = x.shape[1]
        heads = wk.shape[1]
        mean, scale = out_project(att, wo, x, total)
        step = 512
        keys = values = None
        for c in range(width // step):
            cut = slice(c * step, (c + 1) * step)
            d = (total[:, cut] - mean) * scale * gain[layer : layer + 1, cut] + shift[layer : layer + 1, cut]
            d = d.astype(bf16)
            y[:, cut] = d
            k = matmul(d, wk[cut, :])
            v = matmul(d, wv[cut, :])
            keys = k if keys is None else keys + k
            values = v if values is None else values + v
        kv[:, :heads] = keys.astype(bf16)
        kv[:, heads:] = values.astype(bf16)

    when_class(late, run)


def last(layer, att, wo, x, gain, shift, out, total, held, sem):
    half = out.shape[1]
    mean, scale = out_project(att, wo, x, total)
    start = lax.axis_index("tp") * half
    parts = sem.shape[0]
    step = half // parts
    copies = []
    for c in range(parts):
        cut = pl.ds(pl.multiple_of(start + c * step, 128), step)
        g = gain[layer : layer + 1, cut]
        s = shift[layer : layer + 1, cut]
        here = slice(c * step, (c + 1) * step)
        held[:, here] = ((total[:, cut] - mean) * scale * g + s).astype(bf16)
        copy = pltpu.make_async_copy(held.at[:, here], out.at[:, here], sem.at[c])
        copy.start()
        copies.append(copy)
    for copy in copies:
        copy.wait()


def body(tokens, wq, wk, wv, wo, table, gain, shift):
    rows, width = tokens.shape
    cols = wq.shape[2]
    heads = table.shape[1]
    count = lax.axis_size("sp")
    flows = [(s, s + 1) for s in range(count - 1)]
    flat_table = table.reshape(LAYERS * heads, table.shape[2])
    tokens, wq, wk, wv, wo = (
        pltpu.with_memory_space_constraint(a, pltpu.HBM) for a in (tokens, wq, wk, wv, wo)
    )
    kv_shape = ((rows, 2 * cols), bf16)
    x_shape = ((rows, width), bf16)
    q_shape = ((rows, cols), bf16)
    in_shape = (wk.shape[1:], bf16)
    out_shape = (wo.shape[1:], bf16)
    ext = pltpu.VMEM((2 * rows, 2 * cols), bf16)
    total = pltpu.VMEM((rows, width), f32)
    dma = pltpu.SemaphoreType.DMA
    weight = pltpu.VMEM((width, cols), bf16)

    def early_kv(late):
        return kernel_call(
            functools.partial(first_kv, late), [kv_shape, x_shape], [ANY] * 3, (tokens, wk, wv),
            [weight, weight, dma((3, 4))], flops=10**8,
        )

    def send(value, pairs):
        return lax.ppermute(value, "sp", pairs)

    def exchange(att):
        return lax.all_gather(att, "tp", axis=1, tiled=True)

    def flow(late_source):
        return [f for f in flows if late_position(f[0]) == late_source]

    def mid(late, args):
        return kernel_call(
            functools.partial(middle, late, 0), [x_shape, kv_shape], [VM] * 7, args,
            [total], flops=10**8,
        )

    own_late, x_late = early_kv(True)
    prev_late = send(own_late, flow(True))
    own_main, x_main = early_kv(False)
    prev_main = send(own_main, flow(False))
    q, bias, x, out_w, key_w, value_w = kernel_call(
        functools.partial(first_query, 0),
        [q_shape, ((LAYERS * heads * SEG, SPAN), f32), x_shape, out_shape, in_shape, in_shape],
        [VM] * 2 + [ANY] * 4 + [VM], (x_main, x_late, wq, wo, wk, wv, flat_table), [weight, dma((4,))],
    )
    att = kernel_call(
        functools.partial(main_attention, 0), [q_shape], [VM] * 4,
        (q, own_main, prev_late, bias), [ext],
    )[0]
    full = exchange(att)
    x_main, next_main = mid(False, (full, out_w, x, gain, shift, key_w, value_w))
    from_main = send(next_main, flow(False))
    att = kernel_call(
        functools.partial(late_attention, 0), [q_shape], [VM] * 5,
        (q, own_late, prev_main, prev_late, bias), [ext],
    )[0]
    full = exchange(att)
    x_late, next_late = mid(True, (full, out_w, x, gain, shift, key_w, value_w))
    from_late = send(next_late, flow(True))
    q, x, out_w = kernel_call(
        functools.partial(later_query, 1), [q_shape, x_shape, out_shape],
        [VM] * 2 + [ANY] * 2, (x_main, x_late, wq, wo), [weight, dma((2,))],
    )
    att = kernel_call(
        functools.partial(final_attention, 1), [q_shape], [VM] * 6,
        (q, next_main, next_late, from_main, from_late, bias), [ext],
    )[0]
    full = exchange(att)
    return kernel_call(
        functools.partial(last, 1), [((rows, width // 2), bf16)],
        [VM] * 5, (full, out_w, x, gain, shift),
        [total, pltpu.VMEM((rows, width // 2), bf16), dma((4,))], out_specs=[ANY],
    )[0]


def solution(mesh):
    return jax.shard_map(
        body,
        mesh=mesh,
        in_specs=(
            P("sp", None),
            P(None, None, "tp"),
            P(None, None, "tp"),
            P(None, None, "tp"),
            P(),
            P(None, "tp", None),
            P(),
            P(),
        ),
        out_specs=P("sp", "tp"),
        check_vma=False,
    )
```

profile of v0, /device:TPU:513, one launch (start us, length us, event | category | flops | bytes accessed | tf_op | source)
XLA Modules:
  0.0 48.4 jit_solution(11923956889660020733)
XLA Ops:
  0.0 2.3 %shard_map.83 = (bf16[256,512]{1,0:T(8,128)(2,1)S(1)}, bf16[256,2048]{1,0:T(8,128)(2,1)S(1)}) custom-call(bf16[256,2048]{1,0:T(8,128)(2,1)} %tok.3, bf16[2,2048,256]{2,1,0:T(8,128)(2,1)} %wk.5, bf16[2,2048,256]{2,1,0:T(8,128)(2,1)} %wv.5), custom_call_target="tpu_custom_call" | custom-call | flops 100000000 | bytes 1048576 | tf_op jit(solution)/shard_map/pallas_call | solution.py:29
  2.3 0.0 copy-start.2
  2.3 1.3 %collective-permute-start = (bf16[256,512]{1,0:T(8,128)(2,1)S(1)}, bf16[256,512]{1,0:T(8,128)(2,1)S(1)}, u32[]{:S(2)}, u32[]{:S(2)}) collective-permute-start(bf16[256,512]{1,0:T(8,128)(2,1)S(1)} %get-tuple-element.26.own), channel_id=1, source_target_pairs={{2,4},{4,6},{8,10},{12,14},{16,18},{20,22},{24,26},{28,30},{32,34}... | collective-permute-start | bytes 786440 | tf_op jit(solution)/shard_map/ppermute | solution.py:307
  3.6 0.1 shard_map.82
  3.8 1.3 %collective-permute-start.1 = (bf16[256,512]{1,0:T(8,128)(2,1)S(1)}, bf16[256,512]{1,0:T(8,128)(2,1)S(1)}, u32[]{:S(2)}, u32[]{:S(2)}) collective-permute-start(bf16[256,512]{1,0:T(8,128)(2,1)S(1)} %get-tuple-element.25.own), channel_id=1, source_target_pairs={{0,2},{6,8},{10,12},{14,16},{18,20},{22,24},{26,28},{30,32},{34,36... | collective-permute-start | bytes 786440 | tf_op jit(solution)/shard_map/ppermute | solution.py:307
  5.1 0.0 copy-done.2
  5.1 2.5 %shard_map.84 = (bf16[256,256]{1,0:T(8,128)(2,1)S(1)}, f32[512,384]{1,0:T(8,128)S(1)}, bf16[256,2048]{1,0:T(8,128)(2,1)S(1)}, bf16[512,2048]{1,0:T(8,128)(2,1)S(...) custom-call(bf16[256,2048]{1,0:T(8,128)(2,1)S(1)} %get-tuple-element.22.x_main, ...), custom_call_target="tpu_custom_call" | custom-call | flops 1000000000 | bytes 1048576 | tf_op jit(solution)/shard_map/pallas_call | solution.py:29
  7.6 1.2 %collective-permute-done.prev.prev_late = bf16[256,512]{1,0:T(8,128)(2,1)S(1)} collective-permute-done((bf16[256,512]{1,0:T(8,128)(2,1)S(1)}, bf16[256,512]{1,0:T(8,128)(2,1)S(1)}, u32[]{:S(2)}, u32[]{:S(2)}) %collective-permute-start) | collective-permute-done | bytes 262176 | tf_op jit(solution)/shard_map/ppermute | solution.py:307
  8.8 9.4 %collective-permute-done.1.prev_main = bf16[256,512]{1,0:T(8,128)(2,1)S(1)} collective-permute-done((bf16[256,512]{1,0:T(8,128)(2,1)S(1)}, bf16[256,512]{1,0:T(8,128)(2,1)S(1)}, u32[]{:S(2)}, u32[]{:S(2)}) %collective-permute-start.1) | collective-permute-done | bytes 262176 | tf_op jit(solution)/shard_map/ppermute | solution.py:307
  18.3 1.0 %shard_map.87 = bf16[256,256]{1,0:T(8,128)(2,1)S(1)} custom-call(bf16[256,256]{1,0:T(8,128)(2,1)S(1)} %get-tuple-element.24.q, bf16[256,512]{1,0:T(8,128)(2,1)S(1)} %get-tuple-element.26.own, bf16[256,512]{1,0:T(8,128)(2,1)S(1)} %collective-permute-done.1.prev_main, bf16[256,512]{1,0:T(8,128)(2,1)S(1)} %collective-permute-done.prev.prev_late, ...), custom_call_target="tpu_custom_call" | custom-call | flops 1000000000 | bytes 1048576 | tf_op jit(solution)/shard_map/pallas_call | solution.py:29
  19.3 3.2 %all_gather.10.att = bf16[256,512]{1,0:T(8,128)(2,1)S(1)} all-gather(bf16[256,256]{1,0:T(8,128)(2,1)S(1)} %shard_map.87), channel_id=1, replica_groups=mesh['sp'=384,'tp'=2] {'tp'}, dimensions={1}, use_global_device_ids=true | all-gather | bytes 393216 | tf_op jit(solution)/shard_map/all_gather | solution.py:310
  22.4 0.0 copy-start
  22.4 0.0 copy-start.1
  22.4 2.1 %all_gather.9.att = bf16[256,512]{1,0:T(8,128)(2,1)S(1)} all-gather(bf16[256,256]{1,0:T(8,128)(2,1)S(1)} %shard_map.85), channel_id=1, replica_groups=mesh['sp'=384,'tp'=2] {'tp'}, dimensions={1}, use_global_device_ids=true | all-gather | bytes 393216 | tf_op jit(solution)/shard_map/all_gather | solution.py:310
  24.5 0.0 copy-done
  24.5 0.0 copy-done.1
  24.5 1.8 %shard_map.88 = (bf16[256,2048]{1,0:T(8,128)(2,1)S(1)}, bf16[256,512]{1,0:T(8,128)(2,1)S(1)}) custom-call(bf16[256,512]{1,0:T(8,128)(2,1)S(1)} %all_gather.10.att, bf16[512,2048]{1,0:T(8,128)(2,1)S(1)} %get-tuple-element.28.wo, bf16[256,2048]{1,0:T(8,128)(2,1)S(1)} %get-tuple-element.29.x, f32[2,2048]{1,0:T(2,128)S(1)} %copy-done, f32[2,2048]{1,0:T(2,128)S(1)} %copy-done.1, ...), custom_call_target="tpu_custom_call" | custom-call | flops 100000000 | bytes 1048576 | tf_op jit(solution)/shard_map/pallas_call | solution.py:29
  26.4 1.3 %collective-permute-start.3 = (bf16[256,512]{1,0:T(8,128)(2,1)S(1)}, bf16[256,512]{1,0:T(8,128)(2,1)S(1)}, u32[]{:S(2)}, u32[]{:S(2)}) collective-permute-start(bf16[256,512]{1,0:T(8,128)(2,1)S(1)} %get-tuple-element.36.own_late), channel_id=1, source_target_pairs={{2,4},{4,6},{8,10},{12,14},{16,18},{20,22},{24,26},{28,30},{32,34}... | collective-permute-start | bytes 786440 | tf_op jit(solution)/shard_map/ppermute | solution.py:307
  27.7 1.3 %collective-permute-start.2 = (bf16[256,512]{1,0:T(8,128)(2,1)S(1)}, bf16[256,512]{1,0:T(8,128)(2,1)S(1)}, u32[]{:S(2)}, u32[]{:S(2)}) collective-permute-start(bf16[256,512]{1,0:T(8,128)(2,1)S(1)} %get-tuple-element.35.own_main), channel_id=1, source_target_pairs={{0,2},{6,8},{10,12},{14,16},{18,20},{22,24},{26,28},{30,32},{34,36... | collective-permute-start | bytes 786440 | tf_op jit(solution)/shard_map/ppermute | solution.py:307
  29.0 1.9 %shard_map.89 = (bf16[256,256]{1,0:T(8,128)(2,1)S(1)}, bf16[256,2048]{1,0:T(8,128)(2,1)S(1)}, bf16[512,2048]{1,0:T(8,128)(2,1)S(1)}) custom-call(bf16[256,2048]{1,0:T(8,128)(2,1)S(1)} %get-tuple-element.32.x_main, bf16[256,2048]{1,0:T(8,128)(2,1)S(1)} %get-tuple-element.33.x_late, bf16[2,2048,256]{2,1,0:T(8,128)(2,1)} %wq.3, bf16[2,512,2048]{2,1,0:T(8,128)(2,1)} %wo.3), custom_call_target="tpu_custom_call" | custom-call | flops 1000000000 | bytes 1048576 | tf_op jit(solution)/shard_map/pallas_call | solution.py:29
  31.0 2.3 %collective-permute-done.3.prev_late = bf16[256,512]{1,0:T(8,128)(2,1)S(1)} collective-permute-done((bf16[256,512]{1,0:T(8,128)(2,1)S(1)}, bf16[256,512]{1,0:T(8,128)(2,1)S(1)}, u32[]{:S(2)}, u32[]{:S(2)}) %collective-permute-start.3) | collective-permute-done | bytes 262176 | tf_op jit(solution)/shard_map/ppermute | solution.py:307
  33.3 9.3 %collective-permute-done.2.prev_main = bf16[256,512]{1,0:T(8,128)(2,1)S(1)} collective-permute-done((bf16[256,512]{1,0:T(8,128)(2,1)S(1)}, bf16[256,512]{1,0:T(8,128)(2,1)S(1)}, u32[]{:S(2)}, u32[]{:S(2)}) %collective-permute-start.2) | collective-permute-done | bytes 262176 | tf_op jit(solution)/shard_map/ppermute | solution.py:307
  42.5 1.0 %shard_map.90 = bf16[256,256]{1,0:T(8,128)(2,1)S(1)} custom-call(bf16[256,256]{1,0:T(8,128)(2,1)S(1)} %get-tuple-element.34.q, bf16[256,512]{1,0:T(8,128)(2,1)S(1)} %get-tuple-element.35.own_main, bf16[256,512]{1,0:T(8,128)(2,1)S(1)} %get-tuple-element.36.own_late, bf16[256,512]{1,0:T(8,128)(2,1)S(1)} %collective-permute-done.2.prev_main, ...), custom_call_target="tpu_custom_call" | custom-call | flops 1000000000 | bytes 1048576 | tf_op jit(solution)/shard_map/pallas_call | solution.py:29
  43.5 2.8 %all_gather.11.att = bf16[256,512]{1,0:T(8,128)(2,1)S(1)} all-gather(bf16[256,256]{1,0:T(8,128)(2,1)S(1)} %shard_map.90), channel_id=1, replica_groups=mesh['sp'=384,'tp'=2] {'tp'}, dimensions={1}, use_global_device_ids=true | all-gather | bytes 393216 | tf_op jit(solution)/shard_map/all_gather | solution.py:310
  46.4 2.0 %shard_map.91 = bf16[256,1024]{1,0:T(8,128)(2,1)} custom-call(bf16[256,512]{1,0:T(8,128)(2,1)S(1)} %all_gather.11.att, bf16[512,2048]{1,0:T(8,128)(2,1)S(1)} %get-tuple-element.37.wo, bf16[256,2048]{1,0:T(8,128)(2,1)S(1)} %get-tuple-element.38.x, f32[2,2048]{1,0:T(2,128)S(1)} %copy-done, f32[2,2048]{1,0:T(2,128)S(1)} %copy-done.1), custom_call_target="tpu_custom_call" | custom-call | flops 1000000000 | bytes 1048576 | tf_op jit(solution)/shard_map/pallas_call | solution.py:29
  (3 shorter events, 0.0 us)
Async XLA Ops:
  2.3 2.8 %copy-start.2 = (f32[2,4,257]{2,1,0:T(4,128)S(1)}, f32[2,4,257]{2,1,0:T(4,128)}, u32[]{:S(2)}) copy-start(f32[2,4,257]{2,1,0:T(4,128)} %param.13) | copy-start | bytes 24676
  2.3 6.5 %collective-permute-start = (bf16[256,512]{1,0:T(8,128)(2,1)S(1)}, bf16[256,512]{1,0:T(8,128)(2,1)S(1)}, u32[]{:S(2)}, u32[]{:S(2)}) collective-permute-start(bf16[256,512]{1,0:T(8,128)(2,1)S(1)} %get-tuple-element.26.own), channel_id=1, source_target_pairs={{2,4},{4,6},{8,10},{12,14},{16,18},{20,22},{24,26},{28,30},{32,34}... | collective-permute-start | bytes 786440 | tf_op jit(solution)/shard_map/ppermute | solution.py:307
  3.8 14.5 %collective-permute-start.1 = (bf16[256,512]{1,0:T(8,128)(2,1)S(1)}, bf16[256,512]{1,0:T(8,128)(2,1)S(1)}, u32[]{:S(2)}, u32[]{:S(2)}) collective-permute-start(bf16[256,512]{1,0:T(8,128)(2,1)S(1)} %get-tuple-element.25.own), channel_id=1, source_target_pairs={{0,2},{6,8},{10,12},{14,16},{18,20},{22,24},{26,28},{30,32},{34,36... | collective-permute-start | bytes 786440 | tf_op jit(solution)/shard_map/ppermute | solution.py:307
  22.4 2.1 %copy-start = (f32[2,2048]{1,0:T(2,128)S(1)}, f32[2,2048]{1,0:T(2,128)}, u32[]{:S(2)}) copy-start(f32[2,2048]{1,0:T(2,128)} %gain.5) | copy-start | bytes 49156
  22.4 2.1 %copy-start.1 = (f32[2,2048]{1,0:T(2,128)S(1)}, f32[2,2048]{1,0:T(2,128)}, u32[]{:S(2)}) copy-start(f32[2,2048]{1,0:T(2,128)} %shift.5) | copy-start | bytes 49156
  26.4 6.9 %collective-permute-start.3 = (bf16[256,512]{1,0:T(8,128)(2,1)S(1)}, bf16[256,512]{1,0:T(8,128)(2,1)S(1)}, u32[]{:S(2)}, u32[]{:S(2)}) collective-permute-start(bf16[256,512]{1,0:T(8,128)(2,1)S(1)} %get-tuple-element.36.own_late), channel_id=1, source_target_pairs={{2,4},{4,6},{8,10},{12,14},{16,18},{20,22},{24,26},{28,30},{32,34}... | collective-permute-start | bytes 786440 | tf_op jit(solution)/shard_map/ppermute | solution.py:307
  27.7 14.8 %collective-permute-start.2 = (bf16[256,512]{1,0:T(8,128)(2,1)S(1)}, bf16[256,512]{1,0:T(8,128)(2,1)S(1)}, u32[]{:S(2)}, u32[]{:S(2)}) collective-permute-start(bf16[256,512]{1,0:T(8,128)(2,1)S(1)} %get-tuple-element.35.own_main), channel_id=1, source_target_pairs={{0,2},{6,8},{10,12},{14,16},{18,20},{22,24},{26,28},{30,32},{34,36... | collective-permute-start | bytes 786440 | tf_op jit(solution)/shard_map/ppermute | solution.py:307
where the time goes:
time: 48.6 us; the launch traced here: 48.4 us
  waiting for transfers between devices  22.2 us (46%)
  Pallas kernels  12.7 us (26%)
  blocking collectives  8.12 us (17%)
  starting transfers between devices  5.2 us (11%)
    ppermute x4, waiting for transfers between devices, send(): return lax.ppermute(value, 'sp', pairs)  22.2 us
    pallas_call x10, Pallas kernels, kernel_call(): pl.pallas_call(body, out_shape=[jax.ShapeDtypeStruct(s, d) for s, d in ou...  12.7 us
    all_gather x3, blocking collectives, exchange(): return lax.all_gather(att, 'tp', axis=1, tiled=True)  8.12 us
    ppermute x4, starting transfers between devices, send(): return lax.ppermute(value, 'sp', pairs)  5.2 us
  transfers between devices with their start and end apart: 4, of which 4 were waited for; matrix products, arithmetic and copies ran while one was open for 0% of the time, Pallas kernels for 10%

commit v1 on v0

--- a/solution.py
+++ b/solution.py
@@ -12,10 +12,10 @@
 CLIP = 128
 LAYERS = 2
 REACH = LEFT * SEG
-BAND = REACH + SEG
 SPAN = 384
-
-residual_scale = 2.0**0.5
+PART = 256
+
+inverse_residual_scale = 2.0**-0.5
 norm_eps = 1e-05
 masked_score = -1e30
 
@@ -109,10 +109,14 @@
     by_offset = matmul(high, onehot) + matmul(mid, onehot) + matmul(low, onehot)
     far = lax.broadcasted_iota(jnp.int32, (rows, SPAN), 1) <= REACH + SEG - 1 - CLIP
     by_offset = jnp.where(far, t[:, cols - 1 :], by_offset)
+    first = lax.axis_index("sp") == 0
     for r in range(rows):
         line = jnp.broadcast_to(by_offset[r : r + 1, :], (SEG, SPAN))
-        skew = pltpu.roll(line, SPAN - (SEG - 1), 1, stride=1, stride_axis=0)
-        bias[r * SEG : (r + 1) * SEG, :] = skew
+        for place, begin in enumerate((0, 2 * SEG, SEG)):
+            skew = pltpu.roll(line, SPAN - (SEG - 1) - begin, 1, stride=1, stride_axis=0)[:, :PART]
+            if place == 0:
+                skew = jnp.where(first, masked_score, skew)
+            bias[r * SEG : (r + 1) * SEG, place * PART : (place + 1) * PART] = skew
 
 
 def scaled_query(x, w):
@@ -130,51 +134,104 @@
     when_class(True, from_late)
 
 
-def first_query(layer, x_main, x_late, wq, wo, wk, wv, table, q, bias, x, wo0, wk1, wv1, wqs, sem):
+def stacked(q, i, heads):
+    qs = q[i * SEG : (i + 1) * SEG, :]
+    lane = lax.broadcasted_iota(jnp.int32, qs.shape, 1) // (qs.shape[1] // heads)
+    return jnp.concatenate([jnp.where(lane == h, qs, jnp.zeros_like(qs)) for h in range(heads)], axis=0)
+
+
+def by_head(value, width, heads):
+    lane = lax.broadcasted_iota(jnp.int32, (SEG, width), 1) // (width // heads)
+    picked = value[(heads - 1) * SEG :, :]
+    for h in reversed(range(heads - 1)):
+        picked = jnp.where(lane == h, value[h * SEG : (h + 1) * SEG, :], picked)
+    return picked
+
+
+def widened(value, width):
+    return jnp.concatenate([value] * -(-width // 128), axis=1)[:, :width]
+
+
+def scores(stack, keys, bias):
+    return lax.dot_general(stack, keys, (((1,), (1,)), ((), ())), preferred_element_type=f32) + bias
+
+
+def staged(steps):
+    for _ in range(3):
+        for step in steps:
+            next(step)
+
+
+def attend_own(layer, heads, q, own, bias, part, stat):
+    rows, width = q.shape
+    here = slice(layer * heads * SEG, (layer + 1) * heads * SEG)
+
+    def segment(i):
+        known = (i + 1) * SEG
+        table = 2 * PART if i % 2 else PART
+        begin = table + (2 * SEG if i < 2 else 0)
+        score = scores(stacked(q, i, heads), own[:known, :width], bias[here, begin : begin + known])
+        yield
+        peak = jnp.max(score, -1, keepdims=True)
+        expo = jnp.exp(score - peak)
+        lines = slice(i * heads * SEG, (i + 1) * heads * SEG)
+        stat[lines, :128] = jnp.broadcast_to(peak, (heads * SEG, 128))
+        stat[lines, 128:] = jnp.broadcast_to(jnp.sum(expo, -1, keepdims=True), (heads * SEG, 128))
+        expo = expo.astype(bf16)
+        yield
+        part[i * SEG : (i + 1) * SEG, :] = by_head(matmul(expo, own[:known, width:]), width, heads)
+        yield
+
+    staged([segment(i) for i in range(rows // SEG)])
+
+
+def attend_earlier(layer, heads, q, prev, bias, part, stat, out):
+    rows, width = q.shape
+    here = slice(layer * heads * SEG, (layer + 1) * heads * SEG)
+
+    def segment(i):
+        begin = i * SEG
+        score = scores(stacked(q, i, heads), prev[begin:, :width], bias[here, : rows - begin])
+        yield
+        lines = slice(i * heads * SEG, (i + 1) * heads * SEG)
+        own_peak = stat[lines, :128]
+        peak = jnp.maximum(own_peak, jnp.max(score, -1, keepdims=True))
+        expo = jnp.exp(score - widened(peak, rows - begin))
+        kept = jnp.exp(own_peak - peak)
+        scale = inverse_residual_scale / (kept * stat[lines, 128:] + jnp.sum(expo, -1, keepdims=True))
+        expo = expo.astype(bf16)
+        yield
+        mixed = by_head(matmul(expo, prev[begin:, width:]) * widened(scale, width), width, heads)
+        own_mixed = part[i * SEG : (i + 1) * SEG, :] * by_head(widened(kept * scale, width), width, heads)
+        out[i * SEG : (i + 1) * SEG, :] = (mixed + own_mixed).astype(bf16)
+        yield
+
+    staged([segment(i) for i in range(rows // SEG)])
+
+
+def first_query(layer, heads, x_main, x_late, own_main, own_late, wq, wo, wk, wv, table, *rest):
+    q, bias, x, part, stat, wo0, wk1, wv1, wqs, own, sem = rest
     copies = fetch(
         ((wq.at[layer], wqs), (wo.at[layer], wo0), (wk.at[layer + 1], wk1), (wv.at[layer + 1], wv1)), sem
     )
     choose(x_main, x_late, x)
+    choose(own_main, own_late, own)
     fill_bias(table, bias)
     copies[0].wait()
     q[...] = scaled_query(x[...], wqs[...])
+    attend_own(layer, heads, q, own, bias, part, stat)
     for copy in copies[1:]:
         copy.wait()
 
 
-def later_query(layer, x_main, x_late, wq, wo, q, x, wo1, wqs, sem):
+def later_query(layer, heads, x_main, x_late, own_main, own_late, wq, wo, bias, q, x, part, stat, wo1, wqs, own, sem):
     copies = fetch(((wq.at[layer], wqs), (wo.at[layer], wo1)), sem)
     choose(x_main, x_late, x)
+    choose(own_main, own_late, own)
     copies[0].wait()
     q[...] = scaled_query(x[...], wqs[...])
+    attend_own(layer, heads, q, own, bias, part, stat)
     copies[1].wait()
-
-
-def attend(layer, q, bias, ext, out):
-    rows, width = q.shape
-    heads = width // 64
-    lane = lax.broadcasted_iota(jnp.int32, (SEG, width), 1) // 64
-    column = lax.broadcasted_iota(jnp.int32, (1, BAND), 1)
-    blocked = jnp.where(lax.axis_index("sp") == 0, masked_score, 0.0)
-    for i in range(rows // SEG):
-        qs = q[i * SEG : (i + 1) * SEG, :]
-        stack = jnp.concatenate(
-            [jnp.where(lane == h, qs, jnp.zeros_like(qs)) for h in range(heads)], axis=0
-        )
-        keys = ext[i * SEG : i * SEG + BAND, :width]
-        values = ext[i * SEG : i * SEG + BAND, width:]
-        score = lax.dot_general(stack, keys, (((1,), (1,)), ((), ())), preferred_element_type=f32)
-        score = score + bias[layer * heads * SEG : (layer + 1) * heads * SEG, :BAND]
-        score = score + jnp.where(column < REACH - i * SEG, blocked, 0.0)
-        peak = jnp.max(score, -1, keepdims=True)
-        expo = jnp.exp(score - peak)
-        scale = 1.0 / jnp.sum(expo, -1, keepdims=True)
-        mixed = matmul(expo.astype(bf16), values) * scale
-        total = None
-        for h in range(heads):
-            part = jnp.where(lane == h, mixed[h * SEG : (h + 1) * SEG, :], 0.0)
-            total = part if total is None else total + part
-        out[i * SEG : (i + 1) * SEG, :] = total.astype(bf16)
 
 
 def choose_source(main, late, out):
@@ -189,31 +246,21 @@
         out[...] = main[...]
 
 
-def main_attention(layer, q, own, prev, bias, out, ext):
+def main_attention(layer, heads, q, prev, bias, part, stat, out):
+    when_class(False, lambda: attend_earlier(layer, heads, q, prev, bias, part, stat, out))
+
+
+def late_attention(layer, heads, q, prev_main, prev_late, bias, part, stat, out, prev):
     def run():
-        rows = q.shape[0]
-        ext[:rows, :] = prev[...]
-        ext[rows:, :] = own[...]
-        attend(layer, q, bias, ext, out)
-
-    when_class(False, run)
-
-
-def late_attention(layer, q, own, prev_main, prev_late, bias, out, ext):
-    def run():
-        rows = q.shape[0]
-        choose_source(prev_main, prev_late, ext.at[:rows, :])
-        ext[rows:, :] = own[...]
-        attend(layer, q, bias, ext, out)
+        choose_source(prev_main, prev_late, prev)
+        attend_earlier(layer, heads, q, prev, bias, part, stat, out)
 
     when_class(True, run)
 
 
-def final_attention(layer, q, own_main, own_late, prev_main, prev_late, bias, out, ext):
-    rows = q.shape[0]
-    choose(own_main, own_late, ext.at[rows:, :])
-    choose_source(prev_main, prev_late, ext.at[:rows, :])
-    attend(layer, q, bias, ext, out)
+def final_attention(layer, heads, q, prev_main, prev_late, bias, part, stat, out, prev):
+    choose_source(prev_main, prev_late, prev)
+    attend_earlier(layer, heads, q, prev, bias, part, stat, out)
 
 
 def out_project(att, wo, x, total):
@@ -224,7 +271,7 @@
     means, squares = [], []
     for c in range(count):
         cut = slice(c * step, (c + 1) * step)
-        t = residual_scale * x[:, cut].astype(f32) + matmul(a, wo[:, cut])
+        t = x[:, cut].astype(f32) + matmul(a, wo[:, cut])
         total[:, cut] = t
         m = jnp.sum(t, -1, keepdims=True) * (1.0 / step)
         d = t - m
@@ -232,7 +279,7 @@
         squares.append(jnp.sum(d * d, -1, keepdims=True))
     mean = sum(means) * (1.0 / count)
     square = sum(squares) + step * sum((m - mean) * (m - mean) for m in means)
-    return mean, lax.rsqrt(square * (1.0 / width) + norm_eps)
+    return mean, lax.rsqrt(square * (1.0 / width) + norm_eps / 2)
 
 
 def middle(late, layer, att, wo, x, gain, shift, wk, wv, y, kv, total):
@@ -292,7 +339,10 @@
     q_shape = ((rows, cols), bf16)
     in_shape = (wk.shape[1:], bf16)
     out_shape = (wo.shape[1:], bf16)
-    ext = pltpu.VMEM((2 * rows, 2 * cols), bf16)
+    halo = pltpu.VMEM((rows, 2 * cols), bf16)
+    bias_shape = ((LAYERS * heads * SEG, 3 * PART), f32)
+    part_shape = ((rows, cols), f32)
+    stat_shape = ((rows * heads, 256), f32)
     total = pltpu.VMEM((rows, width), f32)
     dma = pltpu.SemaphoreType.DMA
     weight = pltpu.VMEM((width, cols), bf16)
@@ -322,32 +372,34 @@
     prev_late = send(own_late, flow(True))
     own_main, x_main = early_kv(False)
     prev_main = send(own_main, flow(False))
-    q, bias, x, out_w, key_w, value_w = kernel_call(
-        functools.partial(first_query, 0),
-        [q_shape, ((LAYERS * heads * SEG, SPAN), f32), x_shape, out_shape, in_shape, in_shape],
-        [VM] * 2 + [ANY] * 4 + [VM], (x_main, x_late, wq, wo, wk, wv, flat_table), [weight, dma((4,))],
+    q, bias, x, part, stat, out_w, key_w, value_w = kernel_call(
+        functools.partial(first_query, 0, heads),
+        [q_shape, bias_shape, x_shape, part_shape, stat_shape, out_shape, in_shape, in_shape],
+        [VM] * 4 + [ANY] * 4 + [VM], (x_main, x_late, own_main, own_late, wq, wo, wk, wv, flat_table),
+        [weight, halo, dma((4,))],
     )
     att = kernel_call(
-        functools.partial(main_attention, 0), [q_shape], [VM] * 4,
-        (q, own_main, prev_late, bias), [ext],
+        functools.partial(main_attention, 0, heads), [q_shape], [VM] * 5,
+        (q, prev_late, bias, part, stat),
     )[0]
     full = exchange(att)
     x_main, next_main = mid(False, (full, out_w, x, gain, shift, key_w, value_w))
     from_main = send(next_main, flow(False))
     att = kernel_call(
-        functools.partial(late_attention, 0), [q_shape], [VM] * 5,
-        (q, own_late, prev_main, prev_late, bias), [ext],
+        functools.partial(late_attention, 0, heads), [q_shape], [VM] * 6,
+        (q, prev_main, prev_late, bias, part, stat), [halo],
     )[0]
     full = exchange(att)
     x_late, next_late = mid(True, (full, out_w, x, gain, shift, key_w, value_w))
     from_late = send(next_late, flow(True))
-    q, x, out_w = kernel_call(
-        functools.partial(later_query, 1), [q_shape, x_shape, out_shape],
-        [VM] * 2 + [ANY] * 2, (x_main, x_late, wq, wo), [weight, dma((2,))],
+    q, x, part, stat, out_w = kernel_call(
+        functools.partial(later_query, 1, heads),
+        [q_shape, x_shape, part_shape, stat_shape, out_shape], [VM] * 4 + [ANY] * 2 + [VM],
+        (x_main, x_late, next_main, next_late, wq, wo, bias), [weight, halo, dma((2,))],
     )
     att = kernel_call(
-        functools.partial(final_attention, 1), [q_shape], [VM] * 6,
-        (q, next_main, next_late, from_main, from_late, bias), [ext],
+        functools.partial(final_attention, 1, heads), [q_shape], [VM] * 6,
+        (q, from_main, from_late, bias, part, stat), [halo],
     )[0]
     full = exchange(att)
     return kernel_call(

time: 48.6 us -> 47.9 us (0.986)
  waiting for transfers between devices: 22.2 us -> 21.6 us
    ppermute x4, waiting for transfers between devices: 22.2 us -> 21.6 us  [send(): return lax.ppermute(value, 'sp', pairs)]
  transfers between devices with their start and end apart: 4 -> 4, of which waited for: 4 -> 4; matrix products, arithmetic and copies ran while one was open for 0% -> 0% of each run, Pallas kernels for 10% -> 11%
where the time goes in v1:
time: 47.9 us; the launch traced here: 47.6 us
  waiting for transfers between devices  21.6 us (45%)
  Pallas kernels  12.6 us (26%)
  blocking collectives  8.13 us (17%)
  starting transfers between devices  5.2 us (11%)
    ppermute x4, waiting for transfers between devices, send(): return lax.ppermute(value, 'sp', pairs)  21.6 us
    pallas_call x10, Pallas kernels, kernel_call(): pl.pallas_call(body, out_shape=[jax.ShapeDtypeStruct(s, d) for s, d in ou...  12.6 us
    all_gather x3, blocking collectives, exchange(): return lax.all_gather(att, 'tp', axis=1, tiled=True)  8.13 us
    ppermute x4, starting transfers between devices, send(): return lax.ppermute(value, 'sp', pairs)  5.2 us
  transfers between devices with their start and end apart: 4, of which 4 were waited for; matrix products, arithmetic and copies ran while one was open for 0% of the time, Pallas kernels for 11%

profile of v1, /device:TPU:513, one launch (start us, length us, event | category | flops | bytes accessed | tf_op | source)
XLA Modules:
  0.0 47.6 jit_solution(7825987039230919693)
XLA Ops:
  0.0 2.3 %shard_map.83 = (bf16[256,512]{1,0:T(8,128)(2,1)S(1)}, bf16[256,2048]{1,0:T(8,128)(2,1)S(1)}) custom-call(bf16[256,2048]{1,0:T(8,128)(2,1)} %tok.3, bf16[2,2048,256]{2,1,0:T(8,128)(2,1)} %wk.5, bf16[2,2048,256]{2,1,0:T(8,128)(2,1)} %wv.5), custom_call_target="tpu_custom_call" | custom-call | flops 100000000 | bytes 1048576 | tf_op jit(solution)/shard_map/pallas_call | solution.py:29
  2.3 0.0 copy-start.2
  2.3 1.3 %collective-permute-start = (bf16[256,512]{1,0:T(8,128)(2,1)S(1)}, bf16[256,512]{1,0:T(8,128)(2,1)S(1)}, u32[]{:S(2)}, u32[]{:S(2)}) collective-permute-start(bf16[256,512]{1,0:T(8,128)(2,1)S(1)} %get-tuple-element.29.own_late), channel_id=1, source_target_pairs={{2,4},{4,6},{8,10},{12,14},{16,18},{20,22},{24,26},{28,30},{32,34}... | collective-permute-start | bytes 786440 | tf_op jit(solution)/shard_map/ppermute | solution.py:357
  3.6 0.1 shard_map.82
  3.8 1.3 %collective-permute-start.1 = (bf16[256,512]{1,0:T(8,128)(2,1)S(1)}, bf16[256,512]{1,0:T(8,128)(2,1)S(1)}, u32[]{:S(2)}, u32[]{:S(2)}) collective-permute-start(bf16[256,512]{1,0:T(8,128)(2,1)S(1)} %get-tuple-element.28.own_main), channel_id=1, source_target_pairs={{0,2},{6,8},{10,12},{14,16},{18,20},{22,24},{26,28},{30,32},{34,36... | collective-permute-start | bytes 786440 | tf_op jit(solution)/shard_map/ppermute | solution.py:357
  5.1 0.0 copy-done.2
  5.1 2.6 %shard_map.84 = (bf16[256,256]{1,0:T(8,128)(2,1)S(1)}, f32[512,768]{1,0:T(8,128)S(1)}, bf16[256,2048]{1,0:T(8,128)(2,1)S(1)}, f32[256,256]{1,0:T(8,128)S(1)}, f3...) custom-call(bf16[256,2048]{1,0:T(8,128)(2,1)S(1)} %get-tuple-element, ...), custom_call_target="tpu_custom_call" | custom-call | flops 1000000000 | bytes 1048576 | tf_op jit(solution)/shard_map/pallas_call | solution.py:29
  7.7 1.2 %collective-permute-done.prev.prev_late = bf16[256,512]{1,0:T(8,128)(2,1)S(1)} collective-permute-done((bf16[256,512]{1,0:T(8,128)(2,1)S(1)}, bf16[256,512]{1,0:T(8,128)(2,1)S(1)}, u32[]{:S(2)}, u32[]{:S(2)}) %collective-permute-start) | collective-permute-done | bytes 262176 | tf_op jit(solution)/shard_map/ppermute | solution.py:357
  8.8 9.4 %collective-permute-done.1.prev_main = bf16[256,512]{1,0:T(8,128)(2,1)S(1)} collective-permute-done((bf16[256,512]{1,0:T(8,128)(2,1)S(1)}, bf16[256,512]{1,0:T(8,128)(2,1)S(1)}, u32[]{:S(2)}, u32[]{:S(2)}) %collective-permute-start.1) | collective-permute-done | bytes 262176 | tf_op jit(solution)/shard_map/ppermute | solution.py:357
  18.3 0.7 %shard_map.87 = bf16[256,256]{1,0:T(8,128)(2,1)S(1)} custom-call(bf16[256,256]{1,0:T(8,128)(2,1)S(1)} %get-tuple-element.30.q, bf16[256,512]{1,0:T(8,128)(2,1)S(1)} %collective-permute-done.1.prev_main, bf16[256,512]{1,0:T(8,128)(2,1)S(1)} %collective-permute-done.prev.prev_late, f32[512,768]{1,0:T(8,128)S(1)} %get-tuple-element.31.bias, ...), custom_call_target="tpu_custom_call" | custom-call | flops 1000000000 | bytes 1048576 | tf_op jit(solution)/shard_map/pallas_call | solution.py:29
  19.0 3.2 %all_gather.10.att = bf16[256,512]{1,0:T(8,128)(2,1)S(1)} all-gather(bf16[256,256]{1,0:T(8,128)(2,1)S(1)} %shard_map.87), channel_id=1, replica_groups=mesh['sp'=384,'tp'=2] {'tp'}, dimensions={1}, use_global_device_ids=true | all-gather | bytes 393216 | tf_op jit(solution)/shard_map/all_gather | solution.py:360
  22.1 0.0 copy-start
  22.1 0.0 copy-start.1
  22.2 2.1 %all_gather.9.att = bf16[256,512]{1,0:T(8,128)(2,1)S(1)} all-gather(bf16[256,256]{1,0:T(8,128)(2,1)S(1)} %shard_map.85), channel_id=1, replica_groups=mesh['sp'=384,'tp'=2] {'tp'}, dimensions={1}, use_global_device_ids=true | all-gather | bytes 393216 | tf_op jit(solution)/shard_map/all_gather | solution.py:360
  24.3 0.0 copy-done
  24.3 0.0 copy-done.1
  24.3 1.7 %shard_map.88 = (bf16[256,2048]{1,0:T(8,128)(2,1)S(1)}, bf16[256,512]{1,0:T(8,128)(2,1)S(1)}) custom-call(bf16[256,512]{1,0:T(8,128)(2,1)S(1)} %all_gather.10.att, bf16[512,2048]{1,0:T(8,128)(2,1)S(1)} %get-tuple-element.34.wo, bf16[256,2048]{1,0:T(8,128)(2,1)S(1)} %get-tuple-element.35.x, f32[2,2048]{1,0:T(2,128)S(1)} %copy-done, f32[2,2048]{1,0:T(2,128)S(1)} %copy-done.1, ...), custom_call_target="tpu_custom_call" | custom-call | flops 100000000 | bytes 1048576 | tf_op jit(solution)/shard_map/pallas_call | solution.py:29
  26.0 1.3 %collective-permute-start.3 = (bf16[256,512]{1,0:T(8,128)(2,1)S(1)}, bf16[256,512]{1,0:T(8,128)(2,1)S(1)}, u32[]{:S(2)}, u32[]{:S(2)}) collective-permute-start(bf16[256,512]{1,0:T(8,128)(2,1)S(1)} %get-tuple-element.41.own_late), channel_id=1, source_target_pairs={{2,4},{4,6},{8,10},{12,14},{16,18},{20,22},{24,26},{28,30},{32,34}... | collective-permute-start | bytes 786440 | tf_op jit(solution)/shard_map/ppermute | solution.py:357
  27.3 1.3 %collective-permute-start.2 = (bf16[256,512]{1,0:T(8,128)(2,1)S(1)}, bf16[256,512]{1,0:T(8,128)(2,1)S(1)}, u32[]{:S(2)}, u32[]{:S(2)}) collective-permute-start(bf16[256,512]{1,0:T(8,128)(2,1)S(1)} %get-tuple-element.40.own_main), channel_id=1, source_target_pairs={{0,2},{6,8},{10,12},{14,16},{18,20},{22,24},{26,28},{30,32},{34,36... | collective-permute-start | bytes 786440 | tf_op jit(solution)/shard_map/ppermute | solution.py:357
  28.6 2.5 %shard_map.89 = (bf16[256,256]{1,0:T(8,128)(2,1)S(1)}, bf16[256,2048]{1,0:T(8,128)(2,1)S(1)}, f32[256,256]{1,0:T(8,128)S(1)}, f32[1024,256]{1,0:T(8,128)S(1)}, bf16[512,2048]{1,0:T(8,128)(2,1)S(1)}) custom-call(bf16[256,2048]{1,0:T(8,128)(2,1)S(1)} %get-tuple-element.38.x_main, bf16[256,2048]{1,0:T(8,128)(2,1)S(1)} %get-tuple-element.39.x_late, ...), custom_call_target="tpu_custom_call" | custom-call | flops 1000000000 | bytes 1048576 | tf_op jit(solution)/shard_map/pallas_call | solution.py:29
  31.2 1.7 %collective-permute-done.3.prev_late = bf16[256,512]{1,0:T(8,128)(2,1)S(1)} collective-permute-done((bf16[256,512]{1,0:T(8,128)(2,1)S(1)}, bf16[256,512]{1,0:T(8,128)(2,1)S(1)}, u32[]{:S(2)}, u32[]{:S(2)}) %collective-permute-start.3) | collective-permute-done | bytes 262176 | tf_op jit(solution)/shard_map/ppermute | solution.py:357
  32.9 9.3 %collective-permute-done.2.prev_main = bf16[256,512]{1,0:T(8,128)(2,1)S(1)} collective-permute-done((bf16[256,512]{1,0:T(8,128)(2,1)S(1)}, bf16[256,512]{1,0:T(8,128)(2,1)S(1)}, u32[]{:S(2)}, u32[]{:S(2)}) %collective-permute-start.2) | collective-permute-done | bytes 262176 | tf_op jit(solution)/shard_map/ppermute | solution.py:357
  42.1 0.7 %shard_map.90 = bf16[256,256]{1,0:T(8,128)(2,1)S(1)} custom-call(bf16[256,256]{1,0:T(8,128)(2,1)S(1)} %get-tuple-element.42.q, bf16[256,512]{1,0:T(8,128)(2,1)S(1)} %collective-permute-done.2.prev_main, bf16[256,512]{1,0:T(8,128)(2,1)S(1)} %collective-permute-done.3.prev_late, f32[512,768]{1,0:T(8,128)S(1)} %get-tuple-element.31.bias, ...), custom_call_target="tpu_custom_call" | custom-call | flops 1000000000 | bytes 1048576 | tf_op jit(solution)/shard_map/pallas_call | solution.py:29
  42.8 2.9 %all_gather.11.att = bf16[256,512]{1,0:T(8,128)(2,1)S(1)} all-gather(bf16[256,256]{1,0:T(8,128)(2,1)S(1)} %shard_map.90), channel_id=1, replica_groups=mesh['sp'=384,'tp'=2] {'tp'}, dimensions={1}, use_global_device_ids=true | all-gather | bytes 393216 | tf_op jit(solution)/shard_map/all_gather | solution.py:360
  45.7 2.0 %shard_map.91 = bf16[256,1024]{1,0:T(8,128)(2,1)} custom-call(bf16[256,512]{1,0:T(8,128)(2,1)S(1)} %all_gather.11.att, bf16[512,2048]{1,0:T(8,128)(2,1)S(1)} %get-tuple-element.45.wo, bf16[256,2048]{1,0:T(8,128)(2,1)S(1)} %get-tuple-element.46.x, f32[2,2048]{1,0:T(2,128)S(1)} %copy-done, f32[2,2048]{1,0:T(2,128)S(1)} %copy-done.1), custom_call_target="tpu_custom_call" | custom-call | flops 1000000000 | bytes 1048576 | tf_op jit(solution)/shard_map/pallas_call | solution.py:29
  (3 shorter events, 0.0 us)
Async XLA Ops:
  2.3 2.8 %copy-start.2 = (f32[2,4,257]{2,1,0:T(4,128)S(1)}, f32[2,4,257]{2,1,0:T(4,128)}, u32[]{:S(2)}) copy-start(f32[2,4,257]{2,1,0:T(4,128)} %param.13) | copy-start | bytes 24676
  2.3 6.5 %collective-permute-start = (bf16[256,512]{1,0:T(8,128)(2,1)S(1)}, bf16[256,512]{1,0:T(8,128)(2,1)S(1)}, u32[]{:S(2)}, u32[]{:S(2)}) collective-permute-start(bf16[256,512]{1,0:T(8,128)(2,1)S(1)} %get-tuple-element.29.own_late), channel_id=1, source_target_pairs={{2,4},{4,6},{8,10},{12,14},{16,18},{20,22},{24,26},{28,30},{32,34}... | collective-permute-start | bytes 786440 | tf_op jit(solution)/shard_map/ppermute | solution.py:357
  3.8 14.5 %collective-permute-start.1 = (bf16[256,512]{1,0:T(8,128)(2,1)S(1)}, bf16[256,512]{1,0:T(8,128)(2,1)S(1)}, u32[]{:S(2)}, u32[]{:S(2)}) collective-permute-start(bf16[256,512]{1,0:T(8,128)(2,1)S(1)} %get-tuple-element.28.own_main), channel_id=1, source_target_pairs={{0,2},{6,8},{10,12},{14,16},{18,20},{22,24},{26,28},{30,32},{34,36... | collective-permute-start | bytes 786440 | tf_op jit(solution)/shard_map/ppermute | solution.py:357
  22.1 2.1 %copy-start = (f32[2,2048]{1,0:T(2,128)S(1)}, f32[2,2048]{1,0:T(2,128)}, u32[]{:S(2)}) copy-start(f32[2,2048]{1,0:T(2,128)} %gain.5) | copy-start | bytes 49156
  22.1 2.1 %copy-start.1 = (f32[2,2048]{1,0:T(2,128)S(1)}, f32[2,2048]{1,0:T(2,128)}, u32[]{:S(2)}) copy-start(f32[2,2048]{1,0:T(2,128)} %shift.5) | copy-start | bytes 49156
  26.0 6.9 %collective-permute-start.3 = (bf16[256,512]{1,0:T(8,128)(2,1)S(1)}, bf16[256,512]{1,0:T(8,128)(2,1)S(1)}, u32[]{:S(2)}, u32[]{:S(2)}) collective-permute-start(bf16[256,512]{1,0:T(8,128)(2,1)S(1)} %get-tuple-element.41.own_late), channel_id=1, source_target_pairs={{2,4},{4,6},{8,10},{12,14},{16,18},{20,22},{24,26},{28,30},{32,34}... | collective-permute-start | bytes 786440 | tf_op jit(solution)/shard_map/ppermute | solution.py:357
  27.3 14.8 %collective-permute-start.2 = (bf16[256,512]{1,0:T(8,128)(2,1)S(1)}, bf16[256,512]{1,0:T(8,128)(2,1)S(1)}, u32[]{:S(2)}, u32[]{:S(2)}) collective-permute-start(bf16[256,512]{1,0:T(8,128)(2,1)S(1)} %get-tuple-element.40.own_main), channel_id=1, source_target_pairs={{0,2},{6,8},{10,12},{14,16},{18,20},{22,24},{26,28},{30,32},{34,36... | collective-permute-start | bytes 786440 | tf_op jit(solution)/shard_map/ppermute | solution.py:357
